TPU v7x, 512 devices: a 4x2x32 block of a 4x8x32 slice. The times are simulated.
512 devices in a mesh: grp: 2 (over y), sp: 64 (over z, core), tp: 4 (over x).
Axes of the slice: x: 4, y: 2, z: 32, core: 2. Of those that a mesh axis runs over, the one named last changes fastest.
The devices are a block of a 4x8x32 slice.
Arguments:
- tokens: bfloat16 [65536, 2048], P(('grp', 'sp')), parts along dimension 0, may hold values from -6 to 6
- gate_in: bfloat16 [2, 2048, 512], P(None, 'sp', 'tp'), may hold values from -0.125 to 0.125
- gate_conv: bfloat16 [2, 2048, 512], P(None, 'sp', 'tp'), may hold values from -0.125 to 0.125
- value_in: bfloat16 [2, 2048, 512], P(None, 'sp', 'tp'), may hold values from -0.125 to 0.125
- out_weight: bfloat16 [2, 512, 2048], P(None, None, 'sp'), may hold values from -0.25 to 0.25
- conv_taps: float32 [2, 3, 512], replicated, may hold values from -7 to 7
- pre_gain: float32 [2, 2048], replicated, may hold values from 0.1 to 1.9
- mix_gain: float32 [2, 512], replicated, may hold values from 0.1 to 1.9
- post_gain: float32 [2, 2048], replicated, may hold values from 0.1 to 1.9
Outputs:
- result: bfloat16 [65536, 2048], P(('grp', 'sp', 'tp')), parts along dimension 0
There are 2 independent parts, one for each index of `grp`. A program takes and returns all parts, laid end to end along the dimension named above; an argument that names none is the same for every part. Nothing has to cross between parts.
All inputs are finite; a program needn't handle non-finite values.
Results may differ from a plain program's by a relative error of at most 0.011.
Values may be sent and summed in bfloat16 or wider, within the bound.
No kernel may reach another device: no remote copies, remote signals or barrier semaphores. Data moves between devices by JAX's collectives and lax.ppermute only.
A program may use at most 64 MiB of HBM per device.

v0:
```python
import jax
import jax.numpy as jnp
from jax import lax
from jax.sharding import PartitionSpec as P

EPS = 1e-06
GATE_SCALE = 2.0**18
OUT_SCALE = 2.0**17


def passed_along(x, axis, by):
    length = lax.axis_size(axis)
    pairs = [(i, i + by) for i in range(length) if 0 <= i + by < length]
    return lax.ppermute(x, axis, pairs)


def rms_norm(values, gain):
    return values * lax.rsqrt(jnp.mean(values * values, axis=-1, keepdims=True) + EPS) * gain


def stored(values):
    return lax.optimization_barrier(values.astype(jnp.bfloat16))


def sent(values, scale):
    return (values.astype(jnp.float32) * scale).astype(jnp.float16)


def received(values, scale):
    return stored(values.astype(jnp.float32) * (1.0 / scale))


def per_device(
    tokens, gate_in, gate_conv, value_in, out_weight, conv_taps, pre_gain, mix_gain, post_gain
):
    layer_count = gate_in.shape[0]
    channel_count = gate_in.shape[2]
    whole_count = out_weight.shape[1]
    tap_count = conv_taps.shape[1]
    row_count = tokens.shape[0]
    tp_size = lax.axis_size("tp")
    tp_index = lax.axis_index("tp")
    row_share = row_count // tp_size
    pieces = []
    for layer_index in range(layer_count):
        for w in (gate_in, gate_conv, value_in):
            pieces.append(sent(w[layer_index], GATE_SCALE))
        pieces.append(sent(out_weight[layer_index].T, OUT_SCALE))
    packed = jnp.concatenate(pieces, axis=1)
    whole = lax.all_gather(packed, "sp", axis=0, tiled=True)
    stream = tokens.astype(jnp.float32)
    start = 0
    for layer_index in range(layer_count):
        is_last = layer_index == layer_count - 1
        gates = received(whole[:, start : start + 3 * channel_count], GATE_SCALE)
        start += 3 * channel_count
        out_whole = received(whole[:, start : start + whole_count], OUT_SCALE)
        start += whole_count
        normed = stored(rms_norm(stream, pre_gain[layer_index]))
        mixers = stored(jnp.dot(normed, gates, preferred_element_type=jnp.float32))
        outer = mixers[:, :channel_count]
        inner = mixers[:, channel_count : 2 * channel_count]
        values = mixers[:, 2 * channel_count :]
        gated = stored(inner.astype(jnp.float32) * values.astype(jnp.float32))
        before = passed_along(gated[row_count - (tap_count - 1) :], "sp", 1)
        padded = jnp.concatenate([before, gated], axis=0)
        taps_here = lax.dynamic_slice_in_dim(
            conv_taps[layer_index], tp_index * channel_count, channel_count, 1
        )
        filtered = jnp.zeros((row_count, channel_count), jnp.float32)
        for tap_index in range(tap_count):
            filtered = filtered + taps_here[tap_index] * padded[
                tap_index : tap_index + row_count
            ].astype(jnp.float32)
        mixed_raw = stored(outer.astype(jnp.float32) * filtered)
        if is_last:
            arrived = lax.all_to_all(mixed_raw, "tp", split_axis=0, concat_axis=1, tiled=True)
            residual = lax.dynamic_slice_in_dim(stream, tp_index * row_share, row_share, 0)
        else:
            arrived = lax.all_gather(mixed_raw, "tp", axis=1, tiled=True)
            residual = stream
        mixed = stored(rms_norm(arrived.astype(jnp.float32), mix_gain[layer_index]))
        branch = stored(
            lax.dot_general(
                mixed, out_whole, (((1,), (1,)), ((), ())), preferred_element_type=jnp.float32
            )
        )
        stream = residual + rms_norm(branch.astype(jnp.float32), post_gain[layer_index])
    return stream.astype(jnp.bfloat16)


def solution(mesh):
    placed = (
        P(("grp", "sp"), None),
        P(None, "sp", "tp"),
        P(None, "sp", "tp"),
        P(None, "sp", "tp"),
        P(None, None, "sp"),
        P(),
        P(),
        P(),
        P(),
    )
    return jax.shard_map(
        per_device,
        mesh=mesh,
        in_specs=placed,
        out_specs=P(("grp", "sp", "tp"), None),
        check_vma=False,
    )
```

profile of v0, /device:TPU:33, one launch (start us, length us, event | category | flops | bytes accessed | tf_op | source)
XLA Modules:
  0.0 175.5 jit_solution(6006410904357195028)
XLA Ops:
  0.0 0.7 constant_dynamic-update-slice_fusion.5
  0.7 0.7 constant_dynamic-update-slice_fusion.4
  1.4 0.7 constant_dynamic-update-slice_fusion.3
  2.1 0.8 fusion.17
  2.9 0.7 constant_dynamic-update-slice_fusion.2
  3.6 0.7 constant_dynamic-update-slice_fusion.1
  4.3 0.7 constant_dynamic-update-slice_fusion
  5.0 0.8 fusion.19
  5.8 121.4 %all-gather.1 = f16[2048,1792]{1,0:T(8,128)(2,1)S(1)} all-gather(f16[32,1792]{1,0:T(8,128)(2,1)S(1)} %fusion.19), channel_id=1, replica_groups=mesh['grp'=2,'sp'=64,'tp'=4] {'sp'}, dimensions={0}, use_global_device_ids=true | all-gather | bytes 7454720 | tf_op jit(solution)/shard_map/all_gather | solution.py:50
  127.2 1.9 %multiply_convert_fusion.3 = (bf16[2048,384]{1,0:T(8,128)(2,1)}, bf16[2048,384]{1,0:T(8,128)(2,1)S(1)}) fusion(f16[2048,1792]{1,0:T(8,128)(2,1)S(1)} %all-gather.1), kind=kLoop, calls=%fused_computation.14 | loop fusion | flops 4718592 | bytes 6291456 | tf_op jit(solution)/shard_map/convert_element_type | solution.py:22
  129.1 0.0 copy-done.5
  129.1 0.0 copy-done.1
  129.1 0.5 fusion.2
  129.6 0.6 fusion.4
  130.1 1.2 convolution_convert_fusion.3
  131.5 2.3 %collective-permute-start = (bf16[2,128]{1,0:T(2,128)(2,1)S(1)}, bf16[2,128]{1,0:T(2,128)(2,1)S(1)}, u32[]{:S(2)}, u32[]{:S(2)}) collective-permute-start(bf16[2,128]{1,0:T(2,128)(2,1)S(1)} %slice.162), channel_id=1, source_target_pairs={{0,4},{4,8},{8,12},{12,16},{16,20},{20,24},{24,28},{28,32},{32,36}... | collective-permute-start | bytes 1544 | tf_op jit(solution)/shard_map/ppermute | solution.py:14
  133.7 0.0 copy-start.7
  133.7 0.0 copy-start.8
  133.8 0.0 copy-start.6
  133.8 3.0 %multiply_convert_fusion = (bf16[2048,512]{1,0:T(8,128)(2,1)}, bf16[2048,512]{1,0:T(8,128)(2,1)}) fusion(f16[2048,1792]{1,0:T(8,128)(2,1)S(1)} %all-gather.1), kind=kLoop, calls=%fused_computation.10 | loop fusion | flops 6291456 | bytes 8388608 | tf_op jit(solution)/shard_map/convert_element_type | solution.py:22
  136.8 0.0 copy-done.7
  136.8 0.0 copy-done.8
  136.8 0.0 copy-done.6
  136.8 0.0 copy-start.3
  136.9 0.0 collective-permute-done
  136.9 0.1 multiply_convert_fusion.7
  137.0 13.2 %all_gather.7 = bf16[512,512]{1,0:T(8,128)(2,1)S(1)} all-gather(bf16[512,128]{1,0:T(8,128)(2,1)S(1)} %multiply_convert_fusion.7), channel_id=1, replica_groups=mesh['grp'=2,'sp'=64,'tp'=4] {'tp'}, dimensions={1}, use_global_device_ids=true | all-gather | bytes 655360 | tf_op jit(solution)/shard_map/all_gather | solution.py:80
  150.2 0.2 fusion.5
  150.4 0.2 fusion.7
  150.6 1.3 convolution_convert_fusion
  151.9 0.5 fusion
  152.4 1.1 multiply_reduce_fusion
  153.5 0.0 copy-start.4
  153.5 0.4 multiply_convert_fusion.1
  154.0 1.5 copy-done
  155.5 0.6 copy-done.4
  156.1 1.2 convolution_convert_fusion.2
  157.4 4.3 %collective-permute-start.1 = (bf16[2,128]{1,0:T(2,128)(2,1)S(1)}, bf16[2,128]{1,0:T(2,128)(2,1)S(1)}, u32[]{:S(2)}, u32[]{:S(2)}) collective-permute-start(bf16[2,128]{1,0:T(2,128)(2,1)S(1)} %slice.170), channel_id=1, source_target_pairs={{0,4},{4,8},{8,12},{12,16},{16,20},{20,24},{24,28},{28,32},{32,36}... | collective-permute-start | bytes 1544 | tf_op jit(solution)/shard_map/ppermute | solution.py:14
  161.7 0.7 collective-permute-done.1
  162.4 0.1 multiply_convert_fusion.5
  162.5 0.8 copy.10
  163.3 3.4 %all-to-all-start = ((bf16[4,128,128]{1,2,0:T(8,128)(2,1)}), bf16[4,128,128]{1,2,0:T(8,128)(2,1)S(1)}, u32[]{:S(2)}, u32[]{:S(2)}) async-start(bf16[4,128,128]{1,2,0:T(8,128)(2,1)} %copy.10), calls=%async_computation | async-start | bytes 262144 | tf_op jit(solution)/shard_map/all_to_all | solution.py:77
  166.7 5.2 %all-to-all-done = bf16[4,128,128]{1,2,0:T(8,128)(2,1)S(1)} async-done(((bf16[4,128,128]{1,2,0:T(8,128)(2,1)}), bf16[4,128,128]{1,2,0:T(8,128)(2,1)S(1)}, u32[]{:S(2)}, u32[]{:S(2)}) %all-to-all-start) | async-done | bytes 131104 | tf_op jit(solution)/shard_map/all_to_all | solution.py:77
  172.0 0.1 multiply_reduce_fusion.1
  172.1 0.1 fusion.13
  172.2 0.8 convolution_convert_fusion.1
  173.0 0.2 fusion.8
  173.2 2.2 %fusion.11 = bf16[128,2048]{1,0:T(8,128)(2,1)} fusion(bf16[128,2048]{1,0:T(8,128)(2,1)S(1)} %convolution_convert_fusion.1, f32[512,2048]{1,0:T(8,128)} %copy-done, s32[]{:T(128)S(6)} %select_n.2, f32[2048]{0:T(1024)S(1)} %bitcast.72, f32[128]{0:T(128)S(1)} %add_rsqrt_fusion.4), kind=kLoop, calls=%fused_computation.30 | loop fusion | flops 1310720 | bytes 2105860 | tf_op jit(solution)/shard_map/convert_element_type | solution.py:89
  (22 shorter events, 0.2 us)
Async XLA Ops:
  127.2 1.9 %copy-start.5 = (f32[2,2048]{1,0:T(2,128)S(1)}, f32[2,2048]{1,0:T(2,128)}, u32[]{:S(2)}) copy-start(f32[2,2048]{1,0:T(2,128)} %param.15) | copy-start | bytes 49156
  127.2 1.9 %copy-start.1 = (bf16[512,2048]{1,0:T(8,128)(2,1)S(1)}, bf16[512,2048]{1,0:T(8,128)(2,1)}, u32[]{:S(2)}) copy-start(bf16[512,2048]{1,0:T(8,128)(2,1)} %param.9) | copy-start | bytes 6291460
  131.5 5.4 %collective-permute-start = (bf16[2,128]{1,0:T(2,128)(2,1)S(1)}, bf16[2,128]{1,0:T(2,128)(2,1)S(1)}, u32[]{:S(2)}, u32[]{:S(2)}) collective-permute-start(bf16[2,128]{1,0:T(2,128)(2,1)S(1)} %slice.162), channel_id=1, source_target_pairs={{0,4},{4,8},{8,12},{12,16},{16,20},{20,24},{24,28},{28,32},{32,36}... | collective-permute-start | bytes 1544 | tf_op jit(solution)/shard_map/ppermute | solution.py:14
  133.7 3.0 %copy-start.7 = (f32[2,3,512]{2,0,1:T(2,128)S(1)}, f32[2,3,512]{2,0,1:T(2,128)}, u32[]{:S(2)}) copy-start(f32[2,3,512]{2,0,1:T(2,128)} %param.14) | copy-start | bytes 36868
  133.7 3.0 %copy-start.8 = (f32[2,512]{1,0:T(2,128)S(1)}, f32[2,512]{1,0:T(2,128)}, u32[]{:S(2)}) copy-start(f32[2,512]{1,0:T(2,128)} %param.16) | copy-start | bytes 12292
  133.8 3.0 %copy-start.6 = (f32[2,2048]{1,0:T(2,128)S(1)}, f32[2,2048]{1,0:T(2,128)}, u32[]{:S(2)}) copy-start(f32[2,2048]{1,0:T(2,128)} %param.17) | copy-start | bytes 49156
  136.8 13.8 %copy-start.3 = (bf16[2048,512]{1,0:T(8,128)(2,1)S(1)}, bf16[2048,512]{1,0:T(8,128)(2,1)}, u32[]{:S(2)}) copy-start(bf16[2048,512]{1,0:T(8,128)(2,1)} %get-tuple-element.8) | copy-start | bytes 6291460
  153.5 2.0 %copy-start = (f32[512,2048]{1,0:T(8,128)}, f32[512,2048]{1,0:T(8,128)S(1)}, u32[]{:S(2)}) copy-start(f32[512,2048]{1,0:T(8,128)S(1)} %get-tuple-element.6) | copy-start | bytes 12582916
  153.5 2.6 %copy-start.4 = (bf16[2048,384]{1,0:T(8,128)(2,1)S(1)}, bf16[2048,384]{1,0:T(8,128)(2,1)}, u32[]{:S(2)}) copy-start(bf16[2048,384]{1,0:T(8,128)(2,1)} %get-tuple-element.9) | copy-start | bytes 4718596
  156.1 16.1 %copy-start.2 = (bf16[2048,512]{1,0:T(8,128)(2,1)S(1)}, bf16[2048,512]{1,0:T(8,128)(2,1)}, u32[]{:S(2)}) copy-start(bf16[2048,512]{1,0:T(8,128)(2,1)} %get-tuple-element.7) | copy-start | bytes 6291460
  157.4 5.0 %collective-permute-start.1 = (bf16[2,128]{1,0:T(2,128)(2,1)S(1)}, bf16[2,128]{1,0:T(2,128)(2,1)S(1)}, u32[]{:S(2)}, u32[]{:S(2)}) collective-permute-start(bf16[2,128]{1,0:T(2,128)(2,1)S(1)} %slice.170), channel_id=1, source_target_pairs={{0,4},{4,8},{8,12},{12,16},{16,20},{20,24},{24,28},{28,32},{32,36}... | collective-permute-start | bytes 1544 | tf_op jit(solution)/shard_map/ppermute | solution.py:14
  163.3 8.7 %all-to-all-start = ((bf16[4,128,128]{1,2,0:T(8,128)(2,1)}), bf16[4,128,128]{1,2,0:T(8,128)(2,1)S(1)}, u32[]{:S(2)}, u32[]{:S(2)}) async-start(bf16[4,128,128]{1,2,0:T(8,128)(2,1)} %copy.10), calls=%async_computation | async-start | bytes 262144 | tf_op jit(solution)/shard_map/all_to_all | solution.py:77
where the time goes:
time: 176 us; the launch traced here: 175 us
  blocking collectives  135 us (77%)
  other arithmetic  17.1 us (10%)
  starting transfers between devices  9.95 us (6%)
  waiting for transfers between devices  5.92 us (3%)
  matrix products  4.61 us (3%)
  local copies, waits for them, and re-layouts  3.04 us (2%)
    all_gather x1, blocking collectives, per_device(): whole = lax.all_gather(packed, 'sp', axis=0, tiled=True)  121 us
    all_gather x1, blocking collectives, per_device(): arrived = lax.all_gather(mixed_raw, 'tp', axis=1, tiled=True)  13.2 us
    ppermute x2, starting transfers between devices, passed_along(): return lax.ppermute(x, axis, pairs)  6.53 us
    convert_element_type x10, other arithmetic, stored(): return lax.optimization_barrier(values.astype(jnp.bfloat16))  6.5 us
    all_to_all x1, waiting for transfers between devices, per_device(): lax.all_to_all(mixed_raw, 'tp', split_axis=0, concat_axis=1, tiled=True)  5.24 us
    unnamed x7, other arithmetic  5.02 us
  transfers between devices with their start and end apart: 3, of which 2 were waited for; matrix products, arithmetic and copies ran while one was open for 2% of the time, Pallas kernels for 0%

commit v1 on v0

--- a/solution.py
+++ b/solution.py
@@ -1,3 +1,4 @@
+import functools
 import jax
 import jax.numpy as jnp
 from jax import lax
@@ -6,6 +7,16 @@
 EPS = 1e-06
 GATE_SCALE = 2.0**18
 OUT_SCALE = 2.0**17
+
+
+def _report_forms(m, where_dim):
+    x_next = lax.psum(1, "sp")
+    t_next = jnp.stack([m] * x_next)
+    top = lax.all_to_all(t_next, "sp", 0, 0)
+    return jnp.concatenate(top, axis=where_dim)
+
+
+direct_view = functools.partial(_report_forms, where_dim=0)
 
 
 def passed_along(x, axis, by):
@@ -47,7 +58,7 @@
             pieces.append(sent(w[layer_index], GATE_SCALE))
         pieces.append(sent(out_weight[layer_index].T, OUT_SCALE))
     packed = jnp.concatenate(pieces, axis=1)
-    whole = lax.all_gather(packed, "sp", axis=0, tiled=True)
+    whole = direct_view(packed)
     stream = tokens.astype(jnp.float32)
     start = 0
     for layer_index in range(layer_count):

time: 176 us -> 754 us (4.28)
  waiting for transfers between devices: 5.92 us -> 651 us
  blocking collectives: 135 us -> 11.8 us
  starting transfers between devices: 9.95 us -> 57.4 us
    all_to_all x0 -> x1, waiting for transfers between devices: none -> 635 us  [_report_forms(): top = lax.all_to_all(t_next, 'sp', 0, 0)]
    all_gather x1 -> x0, blocking collectives: 121 us -> none  [per_device(): whole = lax.all_gather(packed, 'sp', axis=0, tiled=True)]
    all_to_all x0 -> x1, starting transfers between devices: none -> 47.6 us  [_report_forms(): top = lax.all_to_all(t_next, 'sp', 0, 0)]
    ppermute x2, waiting for transfers between devices: 0.68 us -> 11.8 us  [passed_along(): return lax.ppermute(x, axis, pairs)]
  transfers between devices with their start and end apart: 3 -> 4, of which waited for: 2 -> 4; matrix products, arithmetic and copies ran while one was open for 2% -> 1% of each run, Pallas kernels for 0% -> 0%
where the time goes in v1:
time: 754 us; the launch traced here: 753 us
  waiting for transfers between devices  651 us (86%)
  starting transfers between devices  57.4 us (8%)
  other arithmetic  20.7 us (3%)
  blocking collectives  11.8 us (2%)
    all_to_all x1, waiting for transfers between devices, _report_forms(): top = lax.all_to_all(t_next, 'sp', 0, 0)  635 us
    all_to_all x1, starting transfers between devices, _report_forms(): top = lax.all_to_all(t_next, 'sp', 0, 0)  47.6 us
  transfers between devices with their start and end apart: 4, of which 4 were waited for; matrix products, arithmetic and copies ran while one was open for 1% of the time, Pallas kernels for 0%

profile of v1, /device:TPU:33, one launch (start us, length us, event | category | flops | bytes accessed | tf_op | source)
XLA Modules:
  0.0 752.7 jit_solution(9170751710830120930)
XLA Ops:
  0.0 0.7 constant_dynamic-update-slice_fusion.5
  0.7 0.7 constant_dynamic-update-slice_fusion.4
  1.4 0.7 constant_dynamic-update-slice_fusion.3
  2.1 0.8 fusion.17
  2.9 0.7 constant_dynamic-update-slice_fusion.2
  3.6 0.7 constant_dynamic-update-slice_fusion.1
  4.3 0.7 constant_dynamic-update-slice_fusion
  5.0 0.8 fusion.19
  5.8 3.9 stack.2
  9.7 47.6 %all-to-all-start = ((f16[64,32,1792]{2,1,0:T(8,128)(2,1)}), f16[64,32,1792]{2,1,0:T(8,128)(2,1)}, u32[]{:S(2)}, u32[]{:S(2)}) async-start(f16[64,32,1792]{2,1,0:T(8,128)(2,1)} %stack.2), calls=%async_computation | async-start | bytes 14680064 | tf_op jit(solution)/shard_map/all_to_all | solution.py:15
  57.3 0.0 copy-start.4
  57.3 0.0 copy-done.1
  57.3 0.5 fusion.2
  57.8 0.2 copy-done.4
  58.0 0.0 copy-start.6
  58.1 0.0 copy-start.7
  58.1 0.0 copy-start.5
  58.1 1.9 fusion.4
  59.9 0.0 copy-done.6
  60.0 0.0 copy-done.7
  60.0 0.0 copy-done.5
  60.0 634.7 %all-to-all-done = f16[64,32,1792]{2,1,0:T(8,128)(2,1)} async-done(((f16[64,32,1792]{2,1,0:T(8,128)(2,1)}), f16[64,32,1792]{2,1,0:T(8,128)(2,1)}, u32[]{:S(2)}, u32[]{:S(2)}) %all-to-all-start) | async-done | bytes 7340064 | tf_op jit(solution)/shard_map/all_to_all | solution.py:15
  694.8 2.7 multiply_convert_fusion.3
  697.5 1.2 convolution_convert_fusion.3
  698.8 4.5 collective-permute-start
  703.3 4.5 multiply_convert_fusion
  707.8 5.5 collective-permute-done
  713.3 0.1 multiply_convert_fusion.7
  713.4 11.8 %all_gather.3 = bf16[512,512]{1,0:T(8,128)(2,1)S(1)} all-gather(bf16[512,128]{1,0:T(8,128)(2,1)S(1)} %multiply_convert_fusion.7), channel_id=1, replica_groups=mesh['grp'=2,'sp'=64,'tp'=4] {'tp'}, dimensions={1}, use_global_device_ids=true | all-gather | bytes 655360 | tf_op jit(solution)/shard_map/all_gather | solution.py:91
  725.2 0.2 fusion.5
  725.4 0.2 fusion.7
  725.6 1.3 convolution_convert_fusion
  726.9 0.5 fusion
  727.4 1.1 multiply_reduce_fusion
  728.5 0.4 multiply_convert_fusion.1
  728.9 1.5 copy-done
  730.5 1.2 convolution_convert_fusion.2
  731.8 2.0 collective-permute-start.1
  733.7 6.4 collective-permute-done.1
  740.1 0.1 multiply_convert_fusion.5
  740.2 0.8 copy.10
  741.0 3.4 all-to-all-start.1
  744.4 4.8 all-to-all-done.1
  749.2 0.1 multiply_reduce_fusion.1
  749.3 0.1 fusion.13
  749.4 0.8 convolution_convert_fusion.1
  750.3 0.2 fusion.8
  750.5 2.2 fusion.11
  (22 shorter events, 0.2 us)
Async XLA Ops:
  9.7 47.6 %copy-start.1 = (bf16[512,2048]{1,0:T(8,128)(2,1)S(1)}, bf16[512,2048]{1,0:T(8,128)(2,1)}, u32[]{:S(2)}) copy-start(bf16[512,2048]{1,0:T(8,128)(2,1)} %param.9) | copy-start | bytes 6291460
  9.7 685.1 %all-to-all-start = ((f16[64,32,1792]{2,1,0:T(8,128)(2,1)}), f16[64,32,1792]{2,1,0:T(8,128)(2,1)}, u32[]{:S(2)}, u32[]{:S(2)}) async-start(f16[64,32,1792]{2,1,0:T(8,128)(2,1)} %stack.2), calls=%async_computation | async-start | bytes 14680064 | tf_op jit(solution)/shard_map/all_to_all | solution.py:15
  57.3 0.7 copy-start.4
  58.0 1.9 copy-start.6
  58.1 1.9 copy-start.7
  58.1 1.9 copy-start.5
  694.8 2.7 copy-start.3
  698.8 14.4 %collective-permute-start = (bf16[2,128]{1,0:T(2,128)(2,1)S(1)}, bf16[2,128]{1,0:T(2,128)(2,1)S(1)}, u32[]{:S(2)}, u32[]{:S(2)}) collective-permute-start(bf16[2,128]{1,0:T(2,128)(2,1)S(1)} %slice.162), channel_id=1, source_target_pairs={{0,4},{4,8},{8,12},{12,16},{16,20},{20,24},{24,28},{28,32},{32,36}... | collective-permute-start | bytes 1544 | tf_op jit(solution)/shard_map/ppermute | solution.py:25
  728.5 1.9 copy-start
  730.5 19.0 %copy-start.2 = (bf16[2048,512]{1,0:T(8,128)(2,1)S(1)}, bf16[2048,512]{1,0:T(8,128)(2,1)}, u32[]{:S(2)}) copy-start(bf16[2048,512]{1,0:T(8,128)(2,1)} %get-tuple-element.7) | copy-start | bytes 6291460
  731.8 8.3 %collective-permute-start.1 = (bf16[2,128]{1,0:T(2,128)(2,1)S(1)}, bf16[2,128]{1,0:T(2,128)(2,1)S(1)}, u32[]{:S(2)}, u32[]{:S(2)}) collective-permute-start(bf16[2,128]{1,0:T(2,128)(2,1)S(1)} %slice.170), channel_id=1, source_target_pairs={{0,4},{4,8},{8,12},{12,16},{16,20},{20,24},{24,28},{28,32},{32,36}... | collective-permute-start | bytes 1544 | tf_op jit(solution)/shard_map/ppermute | solution.py:25
  741.0 8.2 %all-to-all-start.1 = ((bf16[4,128,128]{1,2,0:T(8,128)(2,1)}), bf16[4,128,128]{1,2,0:T(8,128)(2,1)S(1)}, u32[]{:S(2)}, u32[]{:S(2)}) async-start(bf16[4,128,128]{1,2,0:T(8,128)(2,1)} %copy.10), calls=%async_computation.1 | async-start | bytes 262144 | tf_op jit(solution)/shard_map/all_to_all | solution.py:88
